TPU v7x, 32 devices: a whole 2x2x4 slice. The times are simulated.
32 devices in a mesh: grp: 2 (over y), sp: 4 (over z), tp: 4 (over x, core).
Axes of the slice: x: 2, y: 2, z: 4, core: 2. Of those that a mesh axis runs over, the one named last changes fastest.
Arguments:
- latent: bfloat16 [2048, 2048], P(('grp', 'sp', 'tp')), parts along dimension 0, may hold values from -6 to 6
- cond: bfloat16 [4096], P(('grp', 'sp')), parts along dimension 0, may hold values from -6 to 6
- context: bfloat16 [512, 2048], P(('grp', 'sp')), parts along dimension 0, may hold values from -6 to 6
- context_cond: bfloat16 [2048], P('sp'), may hold values from -6 to 6
- norm_gain: bfloat16 [2048], replicated, may hold values from 0.099609375 to 1.8984375
- mod_shift: bfloat16 [2048, 2048], P('sp', 'tp'), may hold values from -0.125 to 0.125
- mod_scale: bfloat16 [2048, 2048], P('sp', 'tp'), may hold values from -0.125 to 0.125
- mod_gate: bfloat16 [2048, 2048], P('sp', 'tp'), may hold values from -0.125 to 0.125
- w_query: bfloat16 [2048, 2048], P(None, 'tp'), may hold values from -0.125 to 0.125
- w_key: bfloat16 [2048, 2048], P(None, 'tp'), may hold values from -0.125 to 0.125
- w_value: bfloat16 [2048, 4096], P(None, 'tp'), may hold values from -0.125 to 0.125
- w_gate: bfloat16 [2048, 4096], P(None, 'tp'), may hold values from -0.125 to 0.125
- w_out: bfloat16 [4096, 2048], P('tp'), may hold values from -0.09375 to 0.09375
- decay_rate: float32 [2, 8], P(None, 'tp'), may hold values from 0.00015625 to 0.034
- context_gain: float32 [8], P('tp'), may hold values from 3 to 10
Outputs:
- mixed: bfloat16 [2048, 2048], P(('grp', 'sp', 'tp')), parts along dimension 0
There are 2 independent parts, one for each index of `grp`. A program takes and returns all parts, laid end to end along the dimension named above; an argument that names none is the same for every part. Nothing has to cross between parts.
All inputs are finite; a program needn't handle non-finite values.
Results may differ from a plain program's by a relative error of at most 0.009.
Values may be sent and summed in bfloat16 or wider, within the bound.
A program may use at most 128 MiB of HBM per device.

v0:
```python
import jax
import jax.numpy as jnp
from jax import lax
from jax.sharding import PartitionSpec as P

DK = 256
GRID_W = 128
BLOCK = 128


norm_eps = 1e-06
rope_base = 10000.0
highest = lax.Precision.HIGHEST


def prefix(x, axis, combine, identity, reverse):
    count, here = (lax.axis_size(axis), lax.axis_index(axis))
    everything = jax.tree.map(
        lambda part, kind: lax.all_gather(part.astype(kind), axis), x, (jnp.bfloat16, jnp.bfloat16)
    )
    start = jax.tree.map(
        lambda part, zero: jnp.broadcast_to(jnp.asarray(zero, part.dtype), part.shape), x, identity
    )

    def lap(k, before):
        at = count - 1 - k if reverse else k
        reached = at > here if reverse else at < here
        new = combine(
            before, jax.tree.map(lambda part, own: part[at].astype(own.dtype), everything, x)
        )
        return jax.tree.map(lambda a, b: jnp.where(reached, a, b), new, before)

    return lax.fori_loop(0, count, lap, start)


def modulated(rows, norm_gain, shift, scale):
    values = rows.astype(jnp.float32)
    normed = values * lax.rsqrt(jnp.mean(values * values, axis=-1, keepdims=True) + norm_eps)
    return (normed * norm_gain.astype(jnp.float32) * (1.0 + scale) + shift).astype(jnp.bfloat16)


def rotate(vectors, positions):
    depth = vectors.shape[-1]
    freqs = depth // 4
    inv_freq = rope_base ** (-jnp.arange(freqs, dtype=jnp.float32) / freqs)
    grid_row = (positions // GRID_W).astype(jnp.float32)
    grid_col = (positions % GRID_W).astype(jnp.float32)
    angles = jnp.concatenate([grid_row[:, None] * inv_freq, grid_col[:, None] * inv_freq], axis=-1)[
        :, None, :
    ]
    cos_table = jnp.cos(angles)
    sin_table = jnp.sin(angles)
    first_half, second_half = jnp.split(vectors, 2, axis=-1)
    return jnp.concatenate(
        [
            first_half * cos_table - second_half * sin_table,
            second_half * cos_table + first_half * sin_table,
        ],
        axis=-1,
    )


def context_states(ctx_key, ctx_value, fwd_rate, bwd_rate, context_gain):
    total = ctx_key.shape[0]
    place = jnp.arange(total, dtype=jnp.float32)[:, None]
    fwd_weight = jnp.exp(-fwd_rate[None, :] * (total - 1.0 - place))
    bwd_weight = jnp.exp(-bwd_rate[None, :] * place)
    fwd_keys = (ctx_key.astype(jnp.float32) * fwd_weight[:, :, None]).astype(jnp.bfloat16)
    bwd_keys = (ctx_key.astype(jnp.float32) * bwd_weight[:, :, None]).astype(jnp.bfloat16)
    fwd_state = jnp.einsum("jhd,jhe->hde", fwd_keys, ctx_value, preferred_element_type=jnp.float32)
    bwd_state = jnp.einsum("jhd,jhe->hde", bwd_keys, ctx_value, preferred_element_type=jnp.float32)
    return (fwd_state * context_gain[:, None, None], bwd_state * context_gain[:, None, None])


def join_carry(earlier, later):
    return (earlier[0] * later[1][:, None, None] + later[0], earlier[1] * later[1])


def body(
    latent,
    cond,
    context,
    context_cond,
    norm_gain,
    mod_shift,
    mod_scale,
    mod_gate,
    w_query,
    w_key,
    w_value,
    w_gate,
    w_out,
    decay_rate,
    context_gain,
):
    head_count = w_query.shape[1] // DK
    value_width = w_value.shape[1] // head_count
    local_rows = latent.shape[0]
    span = local_rows * lax.axis_size("tp")
    seq_index = lax.axis_index("sp")
    cond_rows = jax.nn.silu(jnp.stack([cond, context_cond]).astype(jnp.float32)).astype(
        jnp.bfloat16
    )
    shift_part = jnp.dot(cond_rows, mod_shift, preferred_element_type=jnp.float32)
    scale_part = jnp.dot(cond_rows, mod_scale, preferred_element_type=jnp.float32)
    gate_part = jnp.dot(cond_rows[0:1], mod_gate, preferred_element_type=jnp.float32)
    shift_sum, scale_sum, gate_sum = lax.psum((shift_part, scale_part, gate_part), "sp")
    shift, scale, gate = (
        lax.all_gather(shift_sum, "tp", axis=1, tiled=True),
        lax.all_gather(scale_sum, "tp", axis=1, tiled=True),
        lax.all_gather(gate_sum, "tp", axis=1, tiled=True),
    )
    h_latent = modulated(latent, norm_gain, shift[0], scale[0])
    piece = lax.all_gather(h_latent, "tp", axis=0, tiled=True)
    projected = jnp.concatenate(
        [
            jnp.dot(piece, weight, preferred_element_type=jnp.float32)
            for weight in (w_query, w_key, w_value, w_gate)
        ],
        axis=1,
    )
    key_cols = head_count * DK
    val_cols = head_count * value_width
    positions = seq_index * span + jnp.arange(span, dtype=jnp.int32)
    query = rotate(projected[:, :key_cols].reshape(span, head_count, DK), positions).astype(
        jnp.bfloat16
    )
    keys = rotate(
        projected[:, key_cols : 2 * key_cols].reshape(span, head_count, DK) * DK ** (-0.5),
        positions,
    ).astype(jnp.bfloat16)
    values = (
        projected[:, 2 * key_cols : 2 * key_cols + val_cols]
        .astype(jnp.bfloat16)
        .reshape(span, head_count, value_width)
    )
    gate_pre = projected[:, 2 * key_cols + val_cols :].reshape(span, head_count, value_width)
    whole_context = lax.all_gather(context, "sp", axis=0, tiled=True)
    h_context = modulated(whole_context, norm_gain, shift[1], scale[1])
    ctx_key = (jnp.dot(h_context, w_key, preferred_element_type=jnp.float32) * DK ** (-0.5)).astype(
        jnp.bfloat16
    )
    ctx_value = jnp.dot(h_context, w_value, preferred_element_type=jnp.float32).astype(jnp.bfloat16)
    ctx_total = ctx_key.shape[0]
    fwd_rate = decay_rate[0]
    bwd_rate = decay_rate[1]
    ctx_fwd, ctx_bwd = context_states(
        ctx_key.reshape(ctx_total, head_count, DK),
        ctx_value.reshape(ctx_total, head_count, value_width),
        fwd_rate,
        bwd_rate,
        context_gain,
    )
    blocks = span // BLOCK
    query_b = query.reshape(blocks, BLOCK, head_count, DK)
    keys_b = keys.reshape(blocks, BLOCK, head_count, DK)
    values_b = values.reshape(blocks, BLOCK, head_count, value_width)
    place = jnp.arange(BLOCK, dtype=jnp.float32)
    gap = place[:, None] - place[None, :]
    mask = jnp.where(
        gap >= 0, jnp.exp(-fwd_rate[:, None, None] * jnp.maximum(gap, 0.0)), 0.0
    ) + jnp.where(gap <= 0, jnp.exp(-bwd_rate[:, None, None] * jnp.maximum(-gap, 0.0)), 0.0)
    scores = jnp.einsum("bihd,bjhd->bhij", query_b, keys_b, preferred_element_type=jnp.float32)
    weights = (scores * mask[None]).astype(jnp.bfloat16)
    retained = jnp.einsum("bhij,bjhe->bihe", weights, values_b, preferred_element_type=jnp.float32)
    fwd_kw = jnp.exp(-fwd_rate[None, :] * (BLOCK - 1.0 - place[:, None]))
    bwd_kw = jnp.exp(-bwd_rate[None, :] * place[:, None])
    fwd_keys = (keys_b.astype(jnp.float32) * fwd_kw[None, :, :, None]).astype(jnp.bfloat16)
    bwd_keys = (keys_b.astype(jnp.float32) * bwd_kw[None, :, :, None]).astype(jnp.bfloat16)
    fwd_blocks = jnp.einsum(
        "bjhd,bjhe->bhde", fwd_keys, values_b, preferred_element_type=jnp.float32
    )
    bwd_blocks = jnp.einsum(
        "bjhd,bjhe->bhde", bwd_keys, values_b, preferred_element_type=jnp.float32
    )
    order = jnp.arange(blocks, dtype=jnp.float32)
    fwd_local = jnp.einsum(
        "bh,bhde->hde",
        jnp.exp(-fwd_rate[None, :] * BLOCK * (blocks - 1.0 - order[:, None])),
        fwd_blocks,
        precision=highest,
    )
    bwd_local = jnp.einsum(
        "bh,bhde->hde",
        jnp.exp(-bwd_rate[None, :] * BLOCK * order[:, None]),
        bwd_blocks,
        precision=highest,
    )
    unit = jnp.ones((head_count,), jnp.float32)
    blank = jnp.zeros_like(fwd_local)
    fwd_in, fwd_decay = prefix(
        (fwd_local, jnp.exp(-fwd_rate * span)), "sp", join_carry, (blank, unit), False
    )
    bwd_in, bwd_decay = prefix(
        (bwd_local, jnp.exp(-bwd_rate * span)), "sp", join_carry, (blank, unit), True
    )
    fwd_start = fwd_in + fwd_decay[:, None, None] * ctx_fwd
    bwd_start = bwd_in + bwd_decay[:, None, None] * ctx_bwd
    lag = order[:, None] - order[None, :]
    fwd_mix = jnp.where(
        lag[:, :, None] > 0,
        jnp.exp(-fwd_rate[None, None, :] * BLOCK * jnp.maximum(lag - 1.0, 0.0)[:, :, None]),
        0.0,
    )
    bwd_mix = jnp.where(
        lag[:, :, None] < 0,
        jnp.exp(-bwd_rate[None, None, :] * BLOCK * jnp.maximum(-lag - 1.0, 0.0)[:, :, None]),
        0.0,
    )
    fwd_enter = (
        jnp.einsum("cbh,bhde->chde", fwd_mix, fwd_blocks, precision=highest)
        + jnp.exp(-fwd_rate[None, :] * BLOCK * order[:, None])[:, :, None, None] * fwd_start[None]
    )
    bwd_enter = (
        jnp.einsum("cbh,bhde->chde", bwd_mix, bwd_blocks, precision=highest)
        + jnp.exp(-bwd_rate[None, :] * BLOCK * (blocks - 1.0 - order[:, None]))[:, :, None, None]
        * bwd_start[None]
    )
    fwd_qw = jnp.exp(-fwd_rate[None, :] * (place[:, None] + 1.0))[None, :, :, None]
    bwd_qw = jnp.exp(-bwd_rate[None, :] * (BLOCK - place[:, None]))[None, :, :, None]
    fwd_cross = jnp.einsum(
        "bihd,bhde->bihe",
        query_b,
        fwd_enter.astype(jnp.bfloat16),
        preferred_element_type=jnp.float32,
    )
    bwd_cross = jnp.einsum(
        "bihd,bhde->bihe",
        query_b,
        bwd_enter.astype(jnp.bfloat16),
        preferred_element_type=jnp.float32,
    )
    retained = retained + fwd_cross * fwd_qw + bwd_cross * bwd_qw
    retained = retained.reshape(span, head_count, value_width)
    centre = jnp.mean(retained, axis=-1, keepdims=True)
    variance = jnp.mean(jnp.square(retained - centre), axis=-1, keepdims=True)
    normed = (retained - centre) * lax.rsqrt(variance + norm_eps)
    gated = (
        (jax.nn.silu(gate_pre) * normed)
        .astype(jnp.bfloat16)
        .reshape(span, head_count * value_width)
    )
    output_sum = lax.psum_scatter(
        jnp.dot(gated, w_out, preferred_element_type=jnp.float32).astype(jnp.bfloat16),
        "tp",
        scatter_dimension=0,
        tiled=True,
    ).astype(jnp.float32)
    return (latent.astype(jnp.float32) + gate[0] * output_sum).astype(jnp.bfloat16)


def solution(mesh):
    return jax.shard_map(
        body,
        mesh=mesh,
        in_specs=(
            P(("grp", "sp", "tp"), None),
            P(("grp", "sp")),
            P(("grp", "sp"), None),
            P("sp"),
            P(),
            P("sp", "tp"),
            P("sp", "tp"),
            P("sp", "tp"),
            P(None, "tp"),
            P(None, "tp"),
            P(None, "tp"),
            P(None, "tp"),
            P("tp", None),
            P(None, "tp"),
            P("tp"),
        ),
        out_specs=P(("grp", "sp", "tp"), None),
        check_vma=False,
    )
```

profile of v0, /device:TPU:0, one launch (start us, length us, event | category | flops | bytes accessed | tf_op | source)
XLA Modules:
  0.0 266.5 jit_solution(9963465290405761920)
XLA Ops:
  11.7 21.0 %all-reduce = (f32[2,512]{1,0:T(2,128)S(1)}, f32[2,512]{1,0:T(2,128)S(1)}, f32[1,512]{1,0:T(1,128)}) all-reduce(f32[2,512]{1,0:T(2,128)S(1)} %fusion.110, f32[2,512]{1,0:T(2,128)S(1)} %fusion.109, f32[1,512]{1,0:T(1,128)S(1)} %fusion.71), channel_id=1, replica_groups=mesh['grp'=2,'sp'=4,'tp'=4] {'sp'}, use_global_device_ids=true, to_apply=%region_3.4 | all-reduce | flops 2560 | bytes 20480 | tf_op jit(solution)/shard_map/psum | solution.py:107
  32.7 5.2 %all_gather.37 = f32[2,2048]{1,0:T(2,128)S(1)} all-gather(f32[2,512]{1,0:T(2,128)S(1)} %get-tuple-element.376), channel_id=1, replica_groups=mesh['grp'=2,'sp'=4,'tp'=4] {'tp'}, dimensions={1}, use_global_device_ids=true | all-gather | bytes 20480 | tf_op jit(solution)/shard_map/all_gather | solution.py:109
  38.5 5.2 %all_gather.36 = f32[2,2048]{1,0:T(2,128)S(1)} all-gather(f32[2,512]{1,0:T(2,128)S(1)} %get-tuple-element.377), channel_id=1, replica_groups=mesh['grp'=2,'sp'=4,'tp'=4] {'tp'}, dimensions={1}, use_global_device_ids=true | all-gather | bytes 20480 | tf_op jit(solution)/shard_map/all_gather | solution.py:110
  51.3 10.9 %all-gather.9.cloned.1.call-done = bf16[256,2048]{1,0:T(8,128)(2,1)} async-done(((bf16[64,2048]{1,0:T(8,128)(2,1)}), bf16[256,2048]{1,0:T(8,128)(2,1)}) %all-gather.9.cloned.1.call-update) | async-done | bytes 1048592 | tf_op jit(solution)/shard_map/all_gather | solution.py:114
  62.1 3.9 %convolution_convert_fusion.2 = bf16[256,1024]{1,0:T(8,128)(2,1)S(1)} fusion(bf16[256,2048]{1,0:T(8,128)(2,1)} %all-gather.9.cloned.1.call-done, bf16[2048,1024]{1,0:T(8,128)(2,1)} %param.29), kind=kOutput, calls=%fused_computation.44 | convolution fusion | flops 1074003968 | bytes 5767168 | tf_op jit(solution)/shard_map/dot_general | solution.py:117
  69.5 2.8 %convolution_multiply_fusion.3 = f32[256,512]{1,0:T(8,128)} fusion(bf16[256,2048]{1,0:T(8,128)(2,1)} %all-gather.9.cloned.1.call-done, bf16[2048,512]{1,0:T(8,128)(2,1)S(1)} %copy-done), kind=kOutput, calls=%fused_computation.46 | convolution fusion | flops 537001984 | bytes 3670016 | tf_op jit(solution)/shard_map/dot_general | solution.py:117
  77.2 8.3 %fusion.9 = bf16[2,1,256,512]{3,1,2,0:T(2,128)(2,1)S(1)} fusion(f32[2,2,1,1]{0,2,3,1:T(1,128)S(1)} %bitcast.173, f32[2,2,256,512]{3,2,1,0:T(8,128)S(1)} %fusion.42), kind=kOutput, calls=%fused_computation.24 | convolution fusion | flops 6291456 | bytes 2621456 | tf_op jit(solution)/shard_map/bh,bhde->hde/dot_general | solution.py:183
  86.5 11.3 %all-gather.3 = bf16[4,1,2]{2,1,0:T(2,128)(2,1)} all-gather(bf16[1,1,2]{2,1,0:T(2,128)(2,1)S(1)} %copy-done.24), channel_id=1, replica_groups=mesh['grp'=2,'sp'=4,'tp'=4] {'sp'}, dimensions={0}, use_global_device_ids=true | all-gather | bytes 20 | tf_op jit(solution)/shard_map/all_gather | solution.py:19
  97.8 7.8 %all-gather.2 = bf16[4,1,2]{2,1,0:T(2,128)(2,1)} all-gather(bf16[1,1,2]{2,1,0:T(2,128)(2,1)S(1)} %get-tuple-element.402), channel_id=1, replica_groups=mesh['grp'=2,'sp'=4,'tp'=4] {'sp'}, dimensions={0}, use_global_device_ids=true | all-gather | bytes 20 | tf_op jit(solution)/shard_map/all_gather | solution.py:19
  116.5 2.8 %fusion.24 = f32[256,512]{1,0:T(8,128)} fusion(bf16[2048,512]{1,0:T(8,128)(2,1)S(1)} %copy-done, bf16[256,2048]{1,0:T(8,128)(2,1)} %all-gather.11.cloned.1.call-done, f32[2048]{0:T(1024)} %bitcast.168, f32[2048]{0:T(1024)} %bitcast.170, f32[2048]{0:T(1024)S(1)} %convert_element_type.175, f32[256]{0:T(256)S(1)} %add_rsqrt_fusion), kind=kOutput, calls=%fused_computation.48 | convolution fusion | flops 540409856 | bytes 3695616 | tf_op jit(solution)/shard_map/dot_general | solution.py:140
  123.2 8.3 %fusion.12 = bf16[2,1,256,512]{3,1,2,0:T(2,128)(2,1)S(1)} fusion(f32[2,2,1,1]{0,2,3,1:T(1,128)S(1)} %bitcast.172, f32[2,2,256,512]{3,2,1,0:T(8,128)S(1)} %fusion.44), kind=kOutput, calls=%fused_computation.27 | convolution fusion | flops 6291456 | bytes 2621456 | tf_op jit(solution)/shard_map/bh,bhde->hde/dot_general | solution.py:177
  132.5 4.7 %convolution_convert_fusion.1 = bf16[256,1024]{1,0:T(8,128)(2,1)} fusion(bf16[2048,1024]{1,0:T(8,128)(2,1)} %param.29, bf16[256,2048]{1,0:T(8,128)(2,1)} %all-gather.11.cloned.1.call-done, f32[2048]{0:T(1024)} %bitcast.169, f32[2048]{0:T(1024)} %bitcast.171, f32[2048]{0:T(1024)S(1)} %convert_element_type.175, f32[256]{0:T(256)} %copy-done.25), kind=kOutput, calls=%fused_computation.43 | convolution fusion | flops 1077149696 | bytes 5792768 | tf_op jit(solution)/shard_map/dot_general | solution.py:143
  138.4 13.3 %while.35 = (s32[]{:T(128)}, f32[2,256,512]{2,1,0:T(8,128)}, f32[2]{0:T(128)S(1)}, s32[]{:T(128)}, bf16[4,2]{0,1:T(2,128)(2,1)}, /*index=5*/bf16[4,2,256,512]{3,...) while((s32[]{:T(128)}, f32[2,256,512]{2,1,0:T(8,128)}, f32[2]{0:T(128)S(1)}, ...), condition=%wide.region_8.9_spmd.clone, body=%wide.region_7.8_spmd.clone.sunk | while | flops 1310738 | bytes 2621681 | solution.py:33
  142.2 2.6 fusion.133
  145.6 2.7 %fusion.133 = f32[2,256,512]{2,1,0:T(8,128)} fusion(f32[2,256,512]{2,1,0:T(8,128)} %get-tuple-element.514, bf16[4,2,256,512]{3,2,1,0:T(8,128)(2,1)} %get-tuple-element.528, s32[]{:T(128)S(6)} %select_n.190, f32[2]{0:T(128)S(1)} %bitcast_convert_fusion.7, pred[]{:T(512)S(6)} %compare.18, pred[]{:T(512)S(6)} %gt.22), kind=kLoop, calls=%fused_computation.7.clone.1 | loop fusion | flops 1310720 | bytes 2621454 | tf_op jit(solution)/shard_map/while/body/eval_jaxpr/jit(_where)/select_n | solution.py:31
  149.0 2.6 fusion.133
  151.6 32.7 %all-gather.13.cloned.1.call-done = bf16[8,256,512]{2,1,0:T(8,128)(2,1)} async-done(((bf16[2,256,512]{2,1,0:T(8,128)(2,1)}), bf16[8,256,512]{2,1,0:T(8,128)(2,1)}) %all-gather.13.cloned.1.call-update) | async-done | bytes 2097168 | tf_op jit(solution)/shard_map/all_gather | solution.py:19
  184.3 9.2 %while.34 = (s32[]{:T(128)}, f32[2,256,512]{2,1,0:T(8,128)S(1)}, f32[2]{0:T(128)S(1)}, s32[]{:T(128)}, bf16[4,2]{0,1:T(2,128)(2,1)}, /*index=5*/bf16[4,2,256,512]{3,2,1,0:T(8,128)(2,1)}, s32[]{:T(128)}, s32[]{:T(128)}) while((s32[]{:T(128)}, f32[2,256,512]{2,1,0:T(8,128)S(1)}, f32[2]{0:T(128)S(1)}, s32[]{:T(128)}, ...), condition=%wide.region_5.6_spmd.clone, body=%wide.region_4.5_spmd.clone.sunk | while | flops 1310734 | bytes 2621619 | solution.py:33
  197.1 8.8 %fusion.7 = bf16[2,2,256,512]{3,0,2,1:T(2,128)(2,1)S(1)} fusion(f32[2,2,256,512]{3,2,1,0:T(8,128)S(1)} %copy-done.8, f32[2,256,512]{2,1,0:T(8,128)S(1)} %fusion.16, f32[2,2]{0,1:T(2,128)S(1)} %copy-done.27, pred[2,2]{1,0:T(4,128)(4,1)S(1)} %copy-done.37, f32[2,2]{1,0:T(2,128)S(1)} %copy-done.35, f32[2]{0:T(128)S(1)} %copy-done.31), kind=kOutput, calls=%fused_computation.21 | convolution fusion | flops 14155792 | bytes 4194348 | tf_op jit(solution)/shard_map/cbh,bhde->chde/dot_general | solution.py:215
  207.6 9.1 %fusion.8 = bf16[2,2,256,512]{3,0,2,1:T(2,128)(2,1)S(1)} fusion(f32[2,2,256,512]{3,2,1,0:T(8,128)S(1)} %copy-done.10, f32[2,256,512]{2,1,0:T(8,128)S(1)} %fusion.18, f32[2,2]{0,1:T(2,128)S(1)} %copy-done.26, pred[2,2]{1,0:T(4,128)(4,1)S(1)} %copy-done.36, f32[2,2]{1,0:T(2,128)S(1)} %copy-done.34, f32[2]{0:T(128)S(1)} %copy-done.30), kind=kOutput, calls=%fused_computation.23 | convolution fusion | flops 14155792 | bytes 4194348 | tf_op jit(solution)/shard_map/cbh,bhde->chde/dot_general | solution.py:211
  218.2 2.4 fusion.102
  226.5 7.9 %convolution_convert_fusion = bf16[256,2048]{1,0:T(8,128)(2,1)} fusion(bf16[1024,2048]{1,0:T(8,128)(2,1)} %param.31, f32[256,1024]{1,0:T(8,128)S(1)} %bitcast.162, f32[256,1024]{1,0:T(8,128)} %bitcast.163, f32[256,1024]{1,0:T(8,128)} %bitcast.164, bf16[256,2048]{1,0:T(8,128)(2,1)} %all-gather.9.cloned.1.call-done, bf16[2048,1024]{1,0:T(8,128)(2,1)} %param.30), kind=kOutput, calls=%fused_computation.14 | convolution fusion | flops 2150105088 | bytes 13631488 | tf_op jit(solution)/shard_map/dot_general | solution.py:244
  234.5 5.2 %all_gather.35 = f32[1,2048]{1,0:T(1,128)S(1)} all-gather(f32[1,512]{1,0:T(1,128)S(1)} %copy-done.23), channel_id=1, replica_groups=mesh['grp'=2,'sp'=4,'tp'=4] {'tp'}, dimensions={1}, use_global_device_ids=true | all-gather | bytes 10240 | tf_op jit(solution)/shard_map/all_gather | solution.py:111
  239.7 18.6 %reduce-scatter.2.cloned.1.call-done = bf16[64,2048]{1,0:T(8,128)(2,1)} async-done(((bf16[256,2048]{1,0:T(8,128)(2,1)}), bf16[64,2048]{1,0:T(8,128)(2,1)}) %reduce-scatter.2.cloned.1.call-update) | async-done | bytes 262160 | tf_op jit(solution)/shard_map/reduce_scatter | solution.py:243
  (193 shorter events, 68.2 us)
Async XLA Ops:
  6.5 63.0 %copy-start = (bf16[2048,512]{1,0:T(8,128)(2,1)S(1)}, bf16[2048,512]{1,0:T(8,128)(2,1)}, u32[]{:S(2)}) copy-start(bf16[2048,512]{1,0:T(8,128)(2,1)} %param.28) | copy-start | bytes 6291460
  6.5 39.6 %copy-start.4 = (bf16[64,2048]{1,0:T(8,128)(2,1)S(1)}, bf16[64,2048]{1,0:T(8,128)(2,1)}, u32[]{:S(2)}) copy-start(bf16[64,2048]{1,0:T(8,128)(2,1)} %param.19) | copy-start | bytes 786436
  6.5 41.4 %copy-start.21 = (f32[2,2]{1,0:T(2,128)S(1)}, f32[2,2]{1,0:T(2,128)}, u32[]{:S(2)}) copy-start(f32[2,2]{1,0:T(2,128)} %param.32) | copy-start | bytes 52
  6.5 55.6 %all-gather.9.cloned.1.call-start = ((), (), s32[]{:S(2)}) async-start(), calls=%async_computation.1 | async-start | bytes 1310720 | tf_op jit(solution)/shard_map/all_gather | solution.py:114
  47.1 67.4 %all-gather.11.cloned.1.call-start = ((), (), s32[]{:S(2)}) async-start(), calls=%async_computation.2 | async-start | bytes 1310720 | tf_op jit(solution)/shard_map/all_gather | solution.py:138
  47.8 90.6 %all-gather.15.cloned.1.call-start = ((), (), s32[]{:S(2)}) async-start(), calls=%async_computation.5 | async-start | bytes 2621440 | tf_op jit(solution)/shard_map/all_gather | solution.py:19
  48.5 17.5 %copy-start.17 = (f32[2]{0:T(128)}, f32[2]{0:T(128)S(1)}, u32[]{:S(2)}) copy-start(f32[2]{0:T(128)S(1)} %get-tuple-element.403) | copy-start | bytes 28
  48.5 17.5 %copy-start.18 = (f32[2]{0:T(128)}, f32[2]{0:T(128)S(1)}, u32[]{:S(2)}) copy-start(f32[2]{0:T(128)S(1)} %get-tuple-element.404) | copy-start | bytes 28
  62.1 3.9 %copy-start.32 = (bf16[2048,512]{1,0:T(8,128)(2,1)S(1)}, bf16[2048,512]{1,0:T(8,128)(2,1)}, u32[]{:S(2)}) copy-start(bf16[2048,512]{1,0:T(8,128)(2,1)} %param.27) | copy-start | bytes 6291460
  62.1 3.9 %copy-start.33 = (bf16[256,2048]{1,0:T(8,128)(2,1)S(1)}, bf16[256,2048]{1,0:T(8,128)(2,1)}, u32[]{:S(2)}) copy-start(bf16[256,2048]{1,0:T(8,128)(2,1)} %all-gather.9.cloned.1.call-done) | copy-start | bytes 3145732
  67.9 8.6 %copy-start.1 = (bf16[2,128,2,512]{3,2,1,0:T(2,128)(2,1)}, bf16[2,128,2,512]{3,2,1,0:T(2,128)(2,1)S(1)}, u32[]{:S(2)}) copy-start(bf16[2,128,2,512]{3,2,1,0:T(2,128)(2,1)S(1)} %reshape_reshape.3) | copy-start | bytes 1572868
  76.6 8.9 %copy-start.11 = (bf16[256,2,128]{2,0,1:T(8,128)(2,1)}, bf16[256,2,128]{2,0,1:T(8,128)(2,1)S(1)}, u32[]{:S(2)}) copy-start(bf16[256,2,128]{2,0,1:T(8,128)(2,1)S(1)} %get-tuple-element.387) | copy-start | bytes 393220
  76.6 8.9 %copy-start.12 = (bf16[256,2,128]{2,0,1:T(8,128)(2,1)}, bf16[256,2,128]{2,0,1:T(8,128)(2,1)S(1)}, u32[]{:S(2)}) copy-start(bf16[256,2,128]{2,0,1:T(8,128)(2,1)S(1)} %get-tuple-element.388) | copy-start | bytes 393220
  77.1 9.2 %copy-start.7 = (f32[2,2,256,512]{3,2,1,0:T(8,128)}, f32[2,2,256,512]{3,2,1,0:T(8,128)S(1)}, u32[]{:S(2)}) copy-start(f32[2,2,256,512]{3,2,1,0:T(8,128)S(1)} %fusion.42) | copy-start | bytes 6291460
  77.2 9.3 %copy-start.24 = (bf16[1,1,2]{2,1,0:T(2,128)(2,1)S(1)}, bf16[1,1,2]{2,1,0:T(2,128)(2,1)}, u32[]{:S(2)}) copy-start(bf16[1,1,2]{2,1,0:T(2,128)(2,1)} %get-tuple-element.401) | copy-start | bytes 16
  86.4 97.9 %all-gather.13.cloned.1.call-start = ((), (), s32[]{:S(2)}) async-start(), calls=%async_computation.4 | async-start | bytes 2621440 | tf_op jit(solution)/shard_map/all_gather | solution.py:19
  123.2 9.2 %copy-start.9 = (f32[2,2,256,512]{3,2,1,0:T(8,128)}, f32[2,2,256,512]{3,2,1,0:T(8,128)S(1)}, u32[]{:S(2)}) copy-start(f32[2,2,256,512]{3,2,1,0:T(8,128)S(1)} %fusion.44) | copy-start | bytes 6291460
  132.4 125.8 %reduce-scatter.2.cloned.1.call-start = ((), (), s32[]{:S(2)}) async-start(), calls=%async_computation.3 | async-start | bytes 1310720 | tf_op jit(solution)/shard_map/reduce_scatter | solution.py:243
  193.5 2.0 copy-start.2
  193.5 2.0 copy-start.6
  197.1 8.9 %copy-start.5 = (bf16[256,2,128]{2,0,1:T(8,128)(2,1)S(1)}, bf16[256,2,128]{2,0,1:T(8,128)(2,1)}, u32[]{:S(2)}) copy-start(bf16[256,2,128]{2,0,1:T(8,128)(2,1)} %get-tuple-element.380) | copy-start | bytes 393220
  197.1 8.9 %copy-start.20 = (f32[128,2]{0,1:T(2,128)S(1)}, f32[128,2]{0,1:T(2,128)}, u32[]{:S(2)}) copy-start(f32[128,2]{0,1:T(2,128)} %get-tuple-element.411) | copy-start | bytes 3076
  207.6 9.1 %copy-start.19 = (f32[128,2]{0,1:T(2,128)S(1)}, f32[128,2]{0,1:T(2,128)}, u32[]{:S(2)}) copy-start(f32[128,2]{0,1:T(2,128)} %get-tuple-element.420) | copy-start | bytes 3076
  226.5 7.9 %copy-start.23 = (f32[1,512]{1,0:T(1,128)S(1)}, f32[1,512]{1,0:T(1,128)}, u32[]{:S(2)}) copy-start(f32[1,512]{1,0:T(1,128)} %get-tuple-element.378) | copy-start | bytes 6148
  (19 other events, 29.5 us)
Sparse Core Ops, SparseCore 0:
  47.2 14.8 all-gather.8
  63.7 27.9 all-gather.10
  93.3 45.0 all-gather.14
  139.8 44.4 all-gather.12
  234.6 23.6 reduce-scatter.1
where the time goes:
time: 268 us; the launch traced here: 266 us
  matrix products  71.6 us (27%)
  waiting for transfers between devices  64.1 us (24%)
  blocking collectives  55.7 us (21%)
  other arithmetic  33.3 us (12%)
  local copies, waits for them, and re-layouts  27.9 us (10%)
  between operations  13.7 us (5%)
    all_gather x2, waiting for transfers between devices, prefix(): lax.all_gather(part.astype(kind), axis)  33.9 us
    psum x1, blocking collectives, body(): lax.psum((shift_part, scale_part, gate_part), 'sp')  21 us
    all_gather x2, blocking collectives, prefix(): lax.all_gather(part.astype(kind), axis)  19.1 us
    reduce_scatter x1, waiting for transfers between devices, body(): lax.psum_scatter(jnp.dot(gated, w_out, preferred_element_type=jnp.float32...  18.6 us
    select_n x16, other arithmetic, lap(): return jax.tree.map(lambda a, b: jnp.where(reached, a, b), new, before)  16.1 us
    all_gather x1, waiting for transfers between devices, body(): piece = lax.all_gather(h_latent, 'tp', axis=0, tiled=True)  10.9 us
    dot_general x1, matrix products, body(): jnp.einsum('cbh,bhde->chde', fwd_mix, fwd_blocks, precision=highest)  9.06 us
    dot_general x1, matrix products, body(): jnp.einsum('cbh,bhde->chde', bwd_mix, bwd_blocks, precision=highest)  8.8 us
  transfers between devices with their start and end apart: 5, of which 4 were waited for; matrix products, arithmetic and copies ran while one was open for 27% of the time, Pallas kernels for 0%

commit v1 on v0

v1 whole, which is shorter than its diff:
```python
import functools
import math

import jax
import jax.numpy as jnp
from jax import lax
from jax.experimental import pallas as pl
from jax.experimental.pallas import tpu as pltpu
from jax.sharding import PartitionSpec as P

DK = 256
GRID_W = 128
TILE = 256
CHUNK = 64
LAG = 2
norm_eps = 1e-06
rope_base = 10000.0
MESH = pl.DeviceIdType.MESH
F32, BF16 = jnp.float32, jnp.bfloat16


def dot(a, b):
    return jnp.dot(a, b, preferred_element_type=F32)


def dot_tn(a, b):
    return lax.dot_general(a, b, (((0,), (0,)), ((), ())), preferred_element_type=F32)


def dot_nt(a, b):
    return lax.dot_general(a, b, (((1,), (1,)), ((), ())), preferred_element_type=F32)


def remote(src, dst, send, recv, where):
    return pltpu.make_async_remote_copy(
        src_ref=src, dst_ref=dst, send_sem=send, recv_sem=recv, device_id=where, device_id_type=MESH
    )


def rows_of(start, size):
    return pl.ds(pl.multiple_of(start, size), size)


def kernel(
    S,
    T,
    latent,
    cond,
    context,
    norm_gain,
    mod_shift,
    mod_scale,
    mod_gate,
    w_query,
    w_key,
    w_value,
    w_gate,
    w_out,
    decay,
    gain,
    out,
    x_all,
    c_all,
    h_ref,
    hc_ref,
    m_shift,
    m_scale,
    m_gate,
    vq,
    vk,
    vv,
    vg,
    vo,
    m_send,
    m_sp,
    m_tp,
    mod,
    cos_t,
    sin_t,
    q_ref,
    k_ref,
    v_ref,
    ck_ref,
    cv_ref,
    g_ref,
    ret_ref,
    gated,
    loc,
    st_in,
    st_out,
    part,
    p1,
    p2,
    xs,
    xr,
    load_sem,
    lat_send,
    lat_recv,
    ctx_send,
    ctx_fsend,
    ctx_recv,
    msp_send,
    msp_recv,
    mtp_send,
    mtp_recv,
    st_send,
    st_recv,
    p1_send,
    p1_recv,
    p2_send,
    p2_recv,
    x_send,
    x_recv,
):
    sp, tp = lax.axis_index("sp"), lax.axis_index("tp")
    R, D = latent.shape
    Cr = context.shape[0]
    half = Cr // 2
    CT = Cr * S
    span = R * T
    nh = w_query.shape[1] // DK
    DV = w_value.shape[1] // nh
    Mc = mod_shift.shape[1]
    X = T // 2
    chip, core = tp // 2, lax.rem(tp, 2)
    partner = tp + 1 - 2 * core
    is_end = jnp.logical_or(sp == 0, sp == S - 1)
    NC = part.shape[0]
    W = D // NC

    loads = [
        pltpu.make_async_copy(src, dst, load_sem.at[i])
        for i, (src, dst) in enumerate(
            [
                (mod_shift, m_shift),
                (mod_scale, m_scale),
                (mod_gate, m_gate),
                (latent, x_all.at[rows_of(tp * R, R)]),
                (context, c_all.at[rows_of(sp * Cr, Cr)]),
                (w_key, vk),
                (w_value, vv),
                (w_query, vq),
                (w_gate, vg),
                (w_out, vo),
            ]
        )
    ]
    for copy in loads:
        copy.start()

    barrier = pltpu.get_barrier_semaphore()
    for k in range(1, S):
        pl.semaphore_signal(
            barrier, inc=1, device_id={"sp": lax.rem(sp + k, S)}, device_id_type=MESH
        )
    for k in range(1, T):
        pl.semaphore_signal(
            barrier, inc=1, device_id={"tp": lax.rem(tp + k, T)}, device_id_type=MESH
        )
    pl.semaphore_wait(barrier, S + T - 2)

    def lat_copy(src, owner, to, which):
        place = rows_of(owner * R, R)
        return remote(
            latent if src is None else x_all.at[place],
            x_all.at[place],
            lat_send.at[which, to if which == 0 else owner],
            lat_recv.at[owner],
            {"tp": to},
        )

    others = [lax.rem(chip + k, X) for k in range(1, X)]
    direct = [lat_copy(None, tp, 2 * o + core, 0) for o in others] + [
        lat_copy(None, tp, partner, 0)
    ]
    for copy in direct:
        copy.start()

    def ctx_copy(src_ref, owner, part_core, send, recv, where):
        place = rows_of(owner * Cr + part_core * half, half)
        src = context.at[rows_of(part_core * half, half)] if src_ref is None else c_all.at[place]
        return remote(src, c_all.at[place], send, recv, where)

    ends = (0, S - 1)

    def ctx_out(e):
        return ctx_copy(None, sp, core, ctx_send.at[e], ctx_recv.at[0, sp], {"sp": ends[e]})

    for e in range(2):

        @pl.when(sp != ends[e])
        def _():
            ctx_out(e).start()

    for copy in loads[:3]:
        copy.wait()
    rows = cond[...]
    m_send[...] = jnp.zeros_like(m_send)
    m_send[0:2] = dot(rows, m_shift[...])[0:2]
    m_send[2:4] = dot(rows, m_scale[...])[0:2]
    m_send[4:5] = dot(rows, m_gate[...])[0:1]

    def sp_copy(owner, to):
        return remote(m_send, m_sp.at[owner], msp_send.at[to], msp_recv.at[owner], {"sp": to})

    sp_peers = [lax.rem(sp + k, S) for k in range(1, S)]
    tp_peers = [lax.rem(tp + k, T) for k in range(1, T)]
    for p in sp_peers:
        sp_copy(sp, p).start()

    F = DK // 4
    pos = (lax.broadcasted_iota(jnp.int32, (span, 2 * F), 0) + sp * span).astype(F32)
    lane = lax.broadcasted_iota(jnp.int32, (span, 2 * F), 1)
    grid_row = jnp.floor(pos * (1.0 / GRID_W))
    grid_col = pos - grid_row * GRID_W
    freq = jnp.where(lane < F, lane, lane - F).astype(F32)
    angle = jnp.where(lane < F, grid_row, grid_col) * jnp.exp(
        freq * (-math.log(rope_base) / F)
    )
    cos_t[...] = jnp.cos(angle)
    sin_t[...] = jnp.sin(angle)

    total = m_send[...]
    for p in sp_peers:
        sp_copy(p, p).wait_recv()
        total = total + m_sp[p]
    m_tp[tp] = total

    def tp_copy(owner, to):
        return remote(
            m_tp.at[owner], m_tp.at[owner], mtp_send.at[to], mtp_recv.at[owner], {"tp": to}
        )

    for p in tp_peers:
        tp_copy(tp, p).start()

    forwards = []
    for o in others:
        owner = 2 * o + core
        lat_copy(None, owner, owner, 0).wait_recv()
        copy = lat_copy(1, owner, partner, 1)
        copy.start()
        forwards.append(copy)
    loads[3].wait()

    for p in tp_peers:
        tp_copy(p, p).wait_recv()
    for t in range(T):
        mod[:, t * Mc : (t + 1) * Mc] = m_tp[t]

    def modulate(src, dst, start, count, row):
        mult = norm_gain[...].astype(F32) * (1.0 + mod[2 + row : 3 + row, :])
        shift = mod[row : row + 1, :]
        size = min(32, count)

        def lap(i, _):
            place = rows_of(start + i * size, size)
            x = src[place, :].astype(F32)
            scale = lax.rsqrt(jnp.mean(x * x, axis=-1, keepdims=True) + norm_eps)
            dst[place, :] = (x * scale * mult + shift).astype(BF16)
            return 0

        lax.fori_loop(0, count // size, lap, 0)

    modulate(x_all, h_ref, tp * R, R, 0)
    for o in others:
        modulate(x_all, h_ref, (2 * o + core) * R, R, 0)
    lat_copy(None, partner, partner, 0).wait_recv()
    modulate(x_all, h_ref, partner * R, R, 0)
    for o in others:
        owner = 2 * o + 1 - core
        lat_copy(None, owner, owner, 0).wait_recv()
        modulate(x_all, h_ref, owner * R, R, 0)

    scale_k = DK**-0.5

    def rotated(x):
        u, w = x[:, : DK // 2], x[:, DK // 2 :]
        c, s = cos_t[...], sin_t[...]
        return jnp.concatenate([u * c - w * s, w * c + u * s], axis=1).astype(BF16)

    def cols(j, size):
        return pl.ds(pl.multiple_of(j * size, size), size)

    loads[4].wait()

    @pl.when(is_end)
    def _():
        for p in sp_peers:
            ctx_copy(None, p, core, ctx_send.at[0], ctx_recv.at[0, p], {"sp": p}).wait_recv()
            ctx_copy(1, p, core, ctx_fsend.at[p], ctx_recv.at[1, p], {"tp": partner}).start()

    loads[5].wait()

    def key_tile(h, _):
        k_ref[h] = rotated(dot(h_ref[...], vk[:, cols(h, DK)]) * scale_k)
        return 0

    lax.fori_loop(0, nh, key_tile, 0)
    loads[6].wait()

    def value_tile(j, _):
        v_ref[:, cols(j, TILE)] = dot(h_ref[...], vv[:, cols(j, TILE)]).astype(BF16)
        return 0

    lax.fori_loop(0, nh * DV // TILE, value_tile, 0)

    def local_states(h, _):
        k = k_ref[h].astype(F32)
        v = v_ref[:, cols(h, DV)]
        place = lax.broadcasted_iota(jnp.int32, (span, DK), 0).astype(F32)
        fk = (k * jnp.exp(-decay[0, h] * (span - 1.0 - place))).astype(BF16)
        bk = (k * jnp.exp(-decay[1, h] * place)).astype(BF16)
        loc[0, cols(h, DK), :] = dot_tn(fk, v)
        loc[1, cols(h, DK), :] = dot_tn(bk, v)
        return 0

    lax.fori_loop(0, nh, local_states, 0)

    @pl.when(is_end)
    def _():
        for p in sp_peers:
            ctx_copy(
                1, p, 1 - core, ctx_fsend.at[p], ctx_recv.at[1, p], {"tp": partner}
            ).wait_recv()
        modulate(c_all, hc_ref, 0, CT, 1)
        M = min(CT, TILE)
        at_start = sp == 0
        side = jnp.where(at_start, 0, 1)

        def ctx_rows(r, _):
            place = rows_of(r * M, M)

            def ctx_key(h, _):
                ck_ref[h, place, :] = (dot(hc_ref[place, :], vk[:, cols(h, DK)]) * scale_k).astype(
                    BF16
                )
                return 0

            lax.fori_loop(0, nh, ctx_key, 0)

            def ctx_value(j, _):
                cv_ref[place, cols(j, TILE)] = dot(hc_ref[place, :], vv[:, cols(j, TILE)]).astype(
                    BF16
                )
                return 0

            lax.fori_loop(0, nh * DV // TILE, ctx_value, 0)
            return 0

        lax.fori_loop(0, CT // M, ctx_rows, 0)

        def ctx_state(h, _):
            place = lax.broadcasted_iota(jnp.int32, (CT, DK), 0).astype(F32)
            rate = jnp.where(at_start, decay[0, h], decay[1, h])
            away = jnp.where(at_start, CT - 1.0 - place, place)
            keys = (ck_ref[h].astype(F32) * jnp.exp(-rate * away)).astype(BF16)
            state = dot_tn(keys, cv_ref[:, cols(h, DV)]) * gain[h]
            st_in[side, cols(h, DK), :] = state.astype(BF16)
            return 0

        lax.fori_loop(0, nh, ctx_state, 0)

    n = nh * DK // CHUNK
    hop = (sp, S - 1 - sp)
    after = (sp + 1, sp - 1)
    before = (sp - 1, sp + 1)
    per_head = DK // CHUNK

    def st_copy(d, c, to):
        place = rows_of(c * CHUNK, CHUNK)
        return remote(
            st_out.at[d, place],
            st_in.at[d, place],
            st_send.at[d, c],
            st_recv.at[d, c],
            {"sp": to},
        )

    def relay(d, c):
        @pl.when(hop[d] > 0)
        def _():
            st_copy(d, c, before[d]).wait_recv()

        @pl.when(hop[d] < S - 1)
        def _():
            place = rows_of(c * CHUNK, CHUNK)
            fade = jnp.exp(jnp.full((1, DV), -decay[d, c // per_head] * span, F32))
            st_out[d, place, :] = (st_in[d, place, :].astype(F32) * fade + loc[d, place, :]).astype(
                BF16
            )
            st_copy(d, c, after[d]).start()

    ng = nh * DV // TILE
    loads[7].wait()
    loads[8].wait()

    def lap(i, _):
        for d in range(2):
            c = i - LAG * hop[d]

            @pl.when(jnp.logical_and(c >= 0, c < n))
            def _():
                relay(d, c)

        @pl.when(i < nh)
        def _():
            q_ref[i] = rotated(dot(h_ref[...], vq[:, cols(i, DK)]))

        @pl.when(jnp.logical_and(i >= nh, i < nh + ng))
        def _():
            pre = dot(h_ref[...], vg[:, cols(i - nh, TILE)])
            g_ref[:, cols(i - nh, TILE)] = pre / (1.0 + jnp.exp(-pre))

        @pl.when(jnp.logical_and(i >= nh + ng, i < 2 * nh + ng))
        def _():
            h = i - nh - ng
            row = lax.broadcasted_iota(jnp.int32, (span, span), 0)
            col = lax.broadcasted_iota(jnp.int32, (span, span), 1)
            gap = (row - col).astype(F32)
            mask = jnp.where(gap >= 0, jnp.exp(-decay[0, h] * jnp.maximum(gap, 0.0)), 0.0)
            mask += jnp.where(gap <= 0, jnp.exp(-decay[1, h] * jnp.maximum(-gap, 0.0)), 0.0)
            weights = (dot_nt(q_ref[h], k_ref[h]) * mask).astype(BF16)
            ret_ref[h] = dot(weights, v_ref[:, cols(h, DV)])

        return 0

    lax.fori_loop(0, max(n + LAG * (S - 1), 2 * nh + ng), lap, 0)

    def finish(h, _):
        place = lax.broadcasted_iota(jnp.int32, (span, DV), 0).astype(F32)
        q = q_ref[h]
        ret = (
            ret_ref[h]
            + dot(q, st_in[0, cols(h, DK), :]) * jnp.exp(-decay[0, h] * (place + 1.0))
            + dot(q, st_in[1, cols(h, DK), :]) * jnp.exp(-decay[1, h] * (span - place))
        )
        ret = ret - jnp.mean(ret, axis=-1, keepdims=True)
        ret = ret * lax.rsqrt(jnp.mean(ret * ret, axis=-1, keepdims=True) + norm_eps)
        gated[:, cols(h, DV)] = (g_ref[:, cols(h, DV)] * ret).astype(BF16)
        return 0

    lax.fori_loop(0, nh, finish, 0)
    loads[9].wait()

    def p1_copy(c, o):
        return remote(
            part.at[c, 2 * o + 1 - core],
            p1.at[c, o],
            p1_send.at[c, o],
            p1_recv.at[c, o],
            {"tp": partner},
        )

    def p2_copy(c):
        return remote(
            part.at[c, partner], p2.at[c], p2_send.at[c], p2_recv.at[c], {"tp": partner}
        )

    def x_copy(c, owner, o):
        return remote(
            xs.at[c, o], xr.at[c, owner], x_send.at[c, o], x_recv.at[c, owner], {"tp": 2 * o + core}
        )

    def across(c):
        for o in others:
            p1_copy(c, o).wait_recv()
            mine = part[c, 2 * o + core].astype(F32)
            xs[c, o] = (mine + p1[c, o].astype(F32)).astype(BF16)
            x_copy(c, chip, o).start()

    def project(c, _):
        product = dot(gated[...], vo[:, cols(c, W)]).astype(BF16)
        for t in range(T):
            part[c, t] = product[t * R : (t + 1) * R, :]
        for o in others:
            p1_copy(c, o).start()
        p2_copy(c).start()

        @pl.when(c > 0)
        def _():
            across(c - 1)

        return 0

    lax.fori_loop(0, NC, project, 0)
    across(NC - 1)

    def final(c, _):
        p2_copy(c).wait_recv()
        total = part[c, tp].astype(F32) + p2[c].astype(F32)
        for o in others:
            x_copy(c, o, o).wait_recv()
            total = total + xr[c, o].astype(F32)
        mine = x_all[rows_of(tp * R, R), cols(c, W)].astype(F32)
        out[:, cols(c, W)] = (mine + mod[4:5, cols(c, W)] * total).astype(BF16)
        return 0

    lax.fori_loop(0, NC, final, 0)

    for copy in direct + forwards:
        copy.wait_send()
    for e in range(2):

        @pl.when(sp != ends[e])
        def _():
            ctx_out(e).wait_send()

    @pl.when(is_end)
    def _():
        for p in sp_peers:
            ctx_copy(1, p, core, ctx_fsend.at[p], ctx_recv.at[1, p], {"tp": partner}).wait_send()

    for p in sp_peers:
        sp_copy(sp, p).wait_send()
    for p in tp_peers:
        tp_copy(tp, p).wait_send()

    def sent(c, _):
        for d in range(2):

            @pl.when(hop[d] < S - 1)
            def _():
                st_copy(d, c, after[d]).wait_send()

        return 0

    lax.fori_loop(0, n, sent, 0)

    def sent_out(c, _):
        for o in others:
            p1_copy(c, o).wait_send()
            x_copy(c, chip, o).wait_send()
        p2_copy(c).wait_send()
        return 0

    lax.fori_loop(0, NC, sent_out, 0)


def body(
    S,
    T,
    latent,
    cond,
    context,
    context_cond,
    norm_gain,
    mod_shift,
    mod_scale,
    mod_gate,
    w_query,
    w_key,
    w_value,
    w_gate,
    w_out,
    decay_rate,
    context_gain,
):
    R, D = latent.shape
    Cr = context.shape[0]
    span, CT = R * T, Cr * S
    nh = w_query.shape[1] // DK
    DV = w_value.shape[1] // nh
    Mr, Mc = mod_shift.shape
    X = T // 2
    NC = 4
    W = D // NC
    n = nh * DK // CHUNK
    rows = jnp.concatenate(
        [cond[None], context_cond[None], jnp.zeros((14, Mr), cond.dtype)]
    ).astype(F32)
    rows = jax.nn.silu(rows).astype(BF16)
    VMEM = pl.BlockSpec(memory_space=pltpu.VMEM)
    ANY = pl.BlockSpec(memory_space=pl.ANY)
    SMEM = pl.BlockSpec(memory_space=pltpu.SMEM)
    v = pltpu.VMEM
    DMA = pltpu.SemaphoreType.DMA
    return pl.pallas_call(
        functools.partial(kernel, S, T),
        out_shape=jax.ShapeDtypeStruct((R, D), BF16),
        in_specs=[ANY, VMEM, ANY, VMEM] + [ANY] * 8 + [SMEM, SMEM],
        out_specs=VMEM,
        scratch_shapes=[
            v((span, D), BF16),
            v((CT, D), BF16),
            v((span, D), BF16),
            v((CT, D), BF16),
            v((Mr, Mc), BF16),
            v((Mr, Mc), BF16),
            v((Mr, Mc), BF16),
            v(w_query.shape, BF16),
            v(w_key.shape, BF16),
            v(w_value.shape, BF16),
            v(w_gate.shape, BF16),
            v(w_out.shape, BF16),
            v((8, Mc), F32),
            v((S, 8, Mc), F32),
            v((T, 8, Mc), F32),
            v((8, D), F32),
            v((span, DK // 2), F32),
            v((span, DK // 2), F32),
            v((nh, span, DK), BF16),
            v((nh, span, DK), BF16),
            v((span, nh * DV), BF16),
            v((nh, CT, DK), BF16),
            v((CT, nh * DV), BF16),
            v((span, nh * DV), F32),
            v((nh, span, DV), F32),
            v((span, nh * DV), BF16),
            v((2, nh * DK, DV), F32),
            v((2, nh * DK, DV), BF16),
            v((2, nh * DK, DV), BF16),
            v((NC, T, R, W), BF16),
            v((NC, X, R, W), BF16),
            v((NC, R, W), BF16),
            v((NC, X, R, W), BF16),
            v((NC, X, R, W), BF16),
            DMA((10,)),
            DMA((2, T)),
            DMA((T,)),
            DMA((2,)),
            DMA((S,)),
            DMA((2, S)),
            DMA((S,)),
            DMA((S,)),
            DMA((T,)),
            DMA((T,)),
            DMA((2, n)),
            DMA((2, n)),
            DMA((NC, X)),
            DMA((NC, X)),
            DMA((NC,)),
            DMA((NC,)),
            DMA((NC, X)),
            DMA((NC, X)),
        ],
        compiler_params=pltpu.CompilerParams(
            collective_id=0, has_side_effects=True, vmem_limit_bytes=60 * 1024 * 1024
        ),
    )(
        latent,
        rows,
        context,
        norm_gain[None],
        mod_shift,
        mod_scale,
        mod_gate,
        w_query,
        w_key,
        w_value,
        w_gate,
        w_out,
        decay_rate,
        context_gain,
    )


def solution(mesh):
    return jax.shard_map(
        functools.partial(body, mesh.shape["sp"], mesh.shape["tp"]),
        mesh=mesh,
        in_specs=(
            P(("grp", "sp", "tp"), None),
            P(("grp", "sp")),
            P(("grp", "sp"), None),
            P("sp"),
            P(),
            P("sp", "tp"),
            P("sp", "tp"),
            P("sp", "tp"),
            P(None, "tp"),
            P(None, "tp"),
            P(None, "tp"),
            P(None, "tp"),
            P("tp", None),
            P(None, "tp"),
            P("tp"),
        ),
        out_specs=P(("grp", "sp", "tp"), None),
        check_vma=False,
    )
```

time: 268 us -> 68.2 us (0.25)
  matrix products: 71.6 us -> 0 us
  waiting for transfers between devices: 64.1 us -> 0 us
  Pallas kernels: 0 us -> 62.8 us
  blocking collectives: 55.7 us -> 0 us
  other arithmetic: 33.3 us -> 0.69 us
  local copies, waits for them, and re-layouts: 27.9 us -> 4.4 us
  between operations: 13.7 us -> 0.01 us
    dot_general x20 -> x0, matrix products: 71.6 us -> none  [the longest x1 9.06 us: body(): jnp.einsum('cbh,bhde->chde', fwd_mix, fwd_blocks, precision=highest)]
    pallas_call x0 -> x1, Pallas kernels: none -> 62.8 us  [body(): pl.pallas_call(functools.partial(kernel, S, T), out_shape=jax.ShapeDtypeS...]
    all_gather x4 -> x0, waiting for transfers between devices: 44.7 us -> none  [the longest x2 33.9 us: prefix(): lax.all_gather(part.astype(kind), axis)]
    all_gather x5 -> x0, blocking collectives: 34.7 us -> none  [the longest x2 19.1 us: prefix(): lax.all_gather(part.astype(kind), axis)]
    psum x1 -> x0, blocking collectives: 21 us -> none  [body(): lax.psum((shift_part, scale_part, gate_part), 'sp')]
    reduce_scatter x1 -> x0, waiting for transfers between devices: 18.6 us -> none  [body(): lax.psum_scatter(jnp.dot(gated, w_out, preferred_element_type=jnp.float32...]
    select_n x16 -> x0, other arithmetic: 16.1 us -> none  [lap(): return jax.tree.map(lambda a, b: jnp.where(reached, a, b), new, before)]
    dynamic_slice x16 -> x0, local copies, waits for them, and re-layouts: 6.27 us -> none  [lap(): part[at].astype(own.dtype)]
  transfers between devices with their start and end apart: 5 -> 0, of which waited for: 4 -> 0; matrix products, arithmetic and copies ran while one was open for 27% -> 0% of each run, Pallas kernels for 0% -> 0%
where the time goes in v1:
time: 68.2 us; the launch traced here: 67.9 us
  Pallas kernels  62.8 us (92%)
  local copies, waits for them, and re-layouts  4.4 us (6%)
  other arithmetic  0.69 us (1%)
    pallas_call x1, Pallas kernels, body(): pl.pallas_call(functools.partial(kernel, S, T), out_shape=jax.ShapeDtypeS...  62.8 us
    unnamed x1, local copies, waits for them, and re-layouts  1.67 us

profile of v1, /device:TPU:0, one launch (start us, length us, event | category | flops | bytes accessed | tf_op | source)
XLA Modules:
  0.0 67.9 jit_solution(10801270178127905132)
XLA Ops:
  0.0 0.1 pad.2.clone
  0.1 0.7 %broadcast_in_dim.12 = bf16[1,512]{1,0:T(2,128)(2,1)S(1)} reshape(bf16[512]{0:T(512)(128)(2,1)} %param.16) | data formatting | bytes 2048 | tf_op jit(solution)/shard_map/broadcast_in_dim | solution.py:570
  0.8 0.7 %broadcast_in_dim.13 = bf16[1,512]{1,0:T(2,128)(2,1)S(1)} reshape(bf16[512]{0:T(512)(128)(2,1)} %param.18) | data formatting | bytes 2048 | tf_op jit(solution)/shard_map/broadcast_in_dim | solution.py:570
  1.4 1.3 %broadcast_in_dim.15.norm_gain = bf16[1,2048]{1,0:T(2,128)(2,1)} reshape(bf16[2048]{0:T(1024)(128)(2,1)} %param.19) | data formatting | bytes 8192 | tf_op jit(solution)/shard_map/broadcast_in_dim | solution.py:644
  2.7 0.7 %fusion.3.cond = bf16[16,512]{1,0:T(8,128)(2,1)} fusion(bf16[1,512]{1,0:T(2,128)(2,1)S(1)} %broadcast_in_dim.13, bf16[1,512]{1,0:T(2,128)(2,1)S(1)} %broadcast_in_dim.12, bf16[16]{0:T(256)(128)(2,1)S(1)} %pad.2.clone), kind=kLoop, calls=%fused_computation.5 | loop fusion | flops 90112 | bytes 18464 | tf_op jit(solution)/shard_map/convert_element_type | solution.py:572
  3.4 62.8 %shard_map.145 = bf16[64,2048]{1,0:T(8,128)(2,1)} custom-call(bf16[64,2048]{1,0:T(8,128)(2,1)} %latent.1, bf16[16,512]{1,0:T(8,128)(2,1)} %fusion.3.cond, bf16[64,2048]{1,0:T(8,128)(2,1)} %context.1, bf16[1,2048]{1,0:T(2,128)(2,1)} %broadcast_in_dim.15.norm_gain, bf16[512,512]{1,0:T(8,128)(2,1)} %mod_shift.1, bf16[512,512]{1,0:T(8,128)(2,1)} %mod_scale.1, ...), custom_call_target="tpu_custom_call" | custom-call | tf_op jit(solution)/shard_map/pallas_call | solution.py:578
  66.3 1.7 %copy.17 = bf16[64,2048]{1,0:T(8,128)(2,1)} copy(bf16[64,2048]{1,0:T(8,128)(2,1)} %shard_map.145) | data formatting | bytes 524288
  (1 shorter events, 0.0 us)

commit v2 on v1

--- a/solution.py
+++ b/solution.py
@@ -11,7 +11,7 @@
 DK = 256
 GRID_W = 128
 TILE = 256
-CHUNK = 64
+CHUNK = 32
 LAG = 2
 norm_eps = 1e-06
 rope_base = 10000.0
@@ -291,21 +291,21 @@
             ctx_copy(1, p, core, ctx_fsend.at[p], ctx_recv.at[1, p], {"tp": partner}).start()
 
     loads[5].wait()
-
-    def key_tile(h, _):
-        k_ref[h] = rotated(dot(h_ref[...], vk[:, cols(h, DK)]) * scale_k)
-        return 0
-
-    lax.fori_loop(0, nh, key_tile, 0)
     loads[6].wait()
-
-    def value_tile(j, _):
-        v_ref[:, cols(j, TILE)] = dot(h_ref[...], vv[:, cols(j, TILE)]).astype(BF16)
-        return 0
-
-    lax.fori_loop(0, nh * DV // TILE, value_tile, 0)
-
-    def local_states(h, _):
+    M = min(CT, TILE)
+    tiles = DV // TILE
+    at_start = sp == 0
+    side = jnp.where(at_start, 0, 1)
+
+    def latent_head(h):
+        key = rotated(dot(h_ref[...], vk[:, cols(h, DK)]) * scale_k)
+        k_ref[h] = key
+
+        def value_tile(j, _):
+            v_ref[:, cols(j, TILE)] = dot(h_ref[...], vv[:, cols(j, TILE)]).astype(BF16)
+            return 0
+
+        lax.fori_loop(h * tiles, (h + 1) * tiles, value_tile, 0)
         k = k_ref[h].astype(F32)
         v = v_ref[:, cols(h, DV)]
         place = lax.broadcasted_iota(jnp.int32, (span, DK), 0).astype(F32)
@@ -313,9 +313,30 @@
         bk = (k * jnp.exp(-decay[1, h] * place)).astype(BF16)
         loc[0, cols(h, DK), :] = dot_tn(fk, v)
         loc[1, cols(h, DK), :] = dot_tn(bk, v)
-        return 0
-
-    lax.fori_loop(0, nh, local_states, 0)
+
+    def context_head(h):
+        def ctx_rows(r, _):
+            place = rows_of(r * M, M)
+            ck_ref[h, place, :] = (dot(hc_ref[place, :], vk[:, cols(h, DK)]) * scale_k).astype(BF16)
+
+            def ctx_value(j, _):
+                cv_ref[place, cols(j, TILE)] = dot(hc_ref[place, :], vv[:, cols(j, TILE)]).astype(
+                    BF16
+                )
+                return 0
+
+            lax.fori_loop(h * tiles, (h + 1) * tiles, ctx_value, 0)
+            return 0
+
+        lax.fori_loop(0, CT // M, ctx_rows, 0)
+        place = lax.broadcasted_iota(jnp.int32, (CT, DK), 0).astype(F32)
+        rate = jnp.where(at_start, decay[0, h], decay[1, h])
+        away = jnp.where(at_start, CT - 1.0 - place, place)
+        keys = (ck_ref[h].astype(F32) * jnp.exp(-rate * away)).astype(BF16)
+        state = dot_tn(keys, cv_ref[:, cols(h, DV)]) * gain[h]
+        st_in[side, cols(h, DK), :] = state.astype(BF16)
+
+    latent_head(0)
 
     @pl.when(is_end)
     def _():
@@ -324,42 +345,7 @@
                 1, p, 1 - core, ctx_fsend.at[p], ctx_recv.at[1, p], {"tp": partner}
             ).wait_recv()
         modulate(c_all, hc_ref, 0, CT, 1)
-        M = min(CT, TILE)
-        at_start = sp == 0
-        side = jnp.where(at_start, 0, 1)
-
-        def ctx_rows(r, _):
-            place = rows_of(r * M, M)
-
-            def ctx_key(h, _):
-                ck_ref[h, place, :] = (dot(hc_ref[place, :], vk[:, cols(h, DK)]) * scale_k).astype(
-                    BF16
-                )
-                return 0
-
-            lax.fori_loop(0, nh, ctx_key, 0)
-
-            def ctx_value(j, _):
-                cv_ref[place, cols(j, TILE)] = dot(hc_ref[place, :], vv[:, cols(j, TILE)]).astype(
-                    BF16
-                )
-                return 0
-
-            lax.fori_loop(0, nh * DV // TILE, ctx_value, 0)
-            return 0
-
-        lax.fori_loop(0, CT // M, ctx_rows, 0)
-
-        def ctx_state(h, _):
-            place = lax.broadcasted_iota(jnp.int32, (CT, DK), 0).astype(F32)
-            rate = jnp.where(at_start, decay[0, h], decay[1, h])
-            away = jnp.where(at_start, CT - 1.0 - place, place)
-            keys = (ck_ref[h].astype(F32) * jnp.exp(-rate * away)).astype(BF16)
-            state = dot_tn(keys, cv_ref[:, cols(h, DV)]) * gain[h]
-            st_in[side, cols(h, DK), :] = state.astype(BF16)
-            return 0
-
-        lax.fori_loop(0, nh, ctx_state, 0)
+        context_head(0)
 
     n = nh * DK // CHUNK
     hop = (sp, S - 1 - sp)
@@ -395,7 +381,19 @@
     loads[7].wait()
     loads[8].wait()
 
+    inner = max(nh + ng, per_head * (nh - 1) + 1)
+
     def lap(i, _):
+        for h in range(1, nh):
+
+            @pl.when(i == h * per_head)
+            def _():
+                latent_head(h)
+
+                @pl.when(is_end)
+                def _():
+                    context_head(h)
+
         for d in range(2):
             c = i - LAG * hop[d]
 
@@ -412,9 +410,9 @@
             pre = dot(h_ref[...], vg[:, cols(i - nh, TILE)])
             g_ref[:, cols(i - nh, TILE)] = pre / (1.0 + jnp.exp(-pre))
 
-        @pl.when(jnp.logical_and(i >= nh + ng, i < 2 * nh + ng))
-        def _():
-            h = i - nh - ng
+        @pl.when(jnp.logical_and(i >= inner, i < inner + nh))
+        def _():
+            h = i - inner
             row = lax.broadcasted_iota(jnp.int32, (span, span), 0)
             col = lax.broadcasted_iota(jnp.int32, (span, span), 1)
             gap = (row - col).astype(F32)
@@ -425,7 +423,7 @@
 
         return 0
 
-    lax.fori_loop(0, max(n + LAG * (S - 1), 2 * nh + ng), lap, 0)
+    lax.fori_loop(0, max(n + LAG * (S - 1), inner + nh), lap, 0)
 
     def finish(h, _):
         place = lax.broadcasted_iota(jnp.int32, (span, DV), 0).astype(F32)

time: 68.2 us -> 74.7 us (1.095)
  Pallas kernels: 62.8 us -> 69.3 us
    pallas_call x1, Pallas kernels: 62.8 us -> 69.3 us  [body(): pl.pallas_call(functools.partial(kernel, S, T), out_shape=jax.ShapeDtypeS...]
where the time goes in v2:
time: 74.7 us; the launch traced here: 74.4 us
  Pallas kernels  69.3 us (93%)
  local copies, waits for them, and re-layouts  4.4 us (6%)
    pallas_call x1, Pallas kernels, body(): pl.pallas_call(functools.partial(kernel, S, T), out_shape=jax.ShapeDtypeS...  69.3 us
    unnamed x1, local copies, waits for them, and re-layouts  1.67 us

profile of v2, /device:TPU:0, one launch (start us, length us, event | category | flops | bytes accessed | tf_op | source)
XLA Modules:
  0.0 74.4 jit_solution(4977683869356686954)
XLA Ops:
  0.0 0.1 pad.2.clone
  0.1 0.7 broadcast_in_dim.12
  0.8 0.7 broadcast_in_dim.13
  1.4 1.3 %broadcast_in_dim.15.norm_gain = bf16[1,2048]{1,0:T(2,128)(2,1)} reshape(bf16[2048]{0:T(1024)(128)(2,1)} %param.19) | data formatting | bytes 8192 | tf_op jit(solution)/shard_map/broadcast_in_dim | solution.py:642
  2.7 0.7 fusion.3.cond
  3.4 69.3 %shard_map.145 = bf16[64,2048]{1,0:T(8,128)(2,1)} custom-call(bf16[64,2048]{1,0:T(8,128)(2,1)} %latent.1, bf16[16,512]{1,0:T(8,128)(2,1)} %fusion.3.cond, bf16[64,2048]{1,0:T(8,128)(2,1)} %context.1, bf16[1,2048]{1,0:T(2,128)(2,1)} %broadcast_in_dim.15.norm_gain, bf16[512,512]{1,0:T(8,128)(2,1)} %mod_shift.1, bf16[512,512]{1,0:T(8,128)(2,1)} %mod_scale.1, ...), custom_call_target="tpu_custom_call" | custom-call | tf_op jit(solution)/shard_map/pallas_call | solution.py:576
  72.8 1.7 %copy.17 = bf16[64,2048]{1,0:T(8,128)(2,1)} copy(bf16[64,2048]{1,0:T(8,128)(2,1)} %shard_map.145) | data formatting | bytes 524288
  (1 shorter events, 0.0 us)
